TPU v7x, 32 devices: a whole 2x2x4 slice. The times are simulated.
32 devices in a mesh: sp: 4 (over y, x), dp: 8 (over z, core).
Axes of the slice: x: 2, y: 2, z: 4, core: 2. Of those that a mesh axis runs over, the one named last changes fastest.
Arguments:
- tokens: bfloat16 [8, 512, 2048], P('dp', 'sp'), may hold values from -6 to 6
- query_weight: bfloat16 [2048, 1024], P('dp'), may hold values from -0.125 to 0.125
- key_weight: bfloat16 [2048, 1024], P('dp'), may hold values from -0.125 to 0.125
- value_weight: bfloat16 [2048, 2048], P('dp'), may hold values from -0.125 to 0.125
- output_weight: bfloat16 [2048, 2048], P('dp'), may hold values from -0.125 to 0.125
- log_decay: float32 [2, 16], P(None, 'sp'), may hold values from -0.04 to 0, as said below
Outputs:
- mixed: bfloat16 [8, 512, 2048], P('dp', 'sp')
Inputs may be any that keep to these rules, and one draw needn't show every extreme that they name: `log_decay`: every entry is negative: the logarithm of a head's decay per position.
All inputs are finite; a program needn't handle non-finite values.
Results may differ from a plain program's by a relative error of at most 0.012.
Values may be sent and summed in bfloat16 or wider, within the bound.
A program may use at most 128 MiB of HBM per device.

v0:
```python
import functools

import numpy as np
import jax
import jax.numpy as jnp
from jax import lax
from jax.experimental import pallas as pl
from jax.experimental.pallas import tpu as pltpu
from jax.sharding import PartitionSpec as P

HEADS = 16
DK = 64
DV = 128
BLOCK = 512


exact_precision = lax.Precision.HIGHEST


def rotate(values_part, positions):
    half_dim = values_part.shape[-1] // 2
    frequency = 10000.0 ** (-jnp.arange(half_dim, dtype=jnp.float32) / half_dim)
    angles = positions[:, None] * frequency[None, :]
    cosine = jnp.cos(angles)[:, None, :]
    sine_part = jnp.sin(angles)[:, None, :]
    first = values_part[..., :half_dim]
    second = values_part[..., half_dim:]
    return jnp.concatenate(
        [first * cosine - second * sine_part, first * sine_part + second * cosine], axis=-1
    )


def retain(query, key_rows, value_rows, log_rate):
    length, heads, key_dim = query.shape
    value_dim = value_rows.shape[-1]
    count = length // BLOCK
    offsets = jnp.arange(BLOCK, dtype=jnp.float32)
    distance = offsets[:, None] - offsets[None, :]
    decay_inner = jnp.where(
        distance[None] >= 0.0,
        jnp.exp(log_rate[:, None, None] * jnp.maximum(distance, 0.0)[None]),
        0.0,
    )
    decay_query = jnp.exp((offsets[:, None] + 1.0) * log_rate[None, :])[:, :, None]
    decay_key = jnp.exp((BLOCK - 1.0 - offsets)[:, None] * log_rate[None, :])[:, :, None]
    decay_block = jnp.exp(BLOCK * log_rate)[:, None, None]

    def blocks(array):
        return array.reshape(count, BLOCK, heads, array.shape[-1])

    def advance(state, inputs):
        query_block, key_block, value_block = inputs
        inner = (
            jnp.einsum("ihd,jhd->hij", query_block, key_block, preferred_element_type=jnp.float32)
            * decay_inner
        )
        result = jnp.einsum(
            "hij,jhv->ihv",
            inner.astype(jnp.bfloat16),
            value_block,
            preferred_element_type=jnp.float32,
        )
        query_wide = query_block.astype(jnp.float32) * decay_query
        result = result + jnp.einsum("ihd,hdv->ihv", query_wide, state, precision=exact_precision)
        key_wide = key_block.astype(jnp.float32) * decay_key
        state = state * decay_block + jnp.einsum(
            "jhd,jhv->hdv", key_wide, value_block.astype(jnp.float32), precision=exact_precision
        )
        return (state, result)

    initial = jnp.zeros((heads, key_dim, value_dim), jnp.float32)
    final_state, outputs = lax.scan(
        advance, initial, (blocks(query), blocks(key_rows), blocks(value_rows))
    )
    return outputs.reshape(length, heads, value_dim)


def mechanism(stacked, log_decay):
    length = stacked.shape[0]
    widened = stacked[..., : 2 * DK].astype(jnp.float32)
    positions = jnp.arange(length, dtype=jnp.float32)
    query = rotate(widened[..., :DK], positions).astype(jnp.bfloat16)
    key_rows = rotate(widened[..., DK : 2 * DK], positions).astype(jnp.bfloat16)
    value_rows = stacked[..., 2 * DK :]
    forward = retain(query, key_rows, value_rows, log_decay[0])
    backward = retain(
        jnp.flip(query, 0), jnp.flip(key_rows, 0), jnp.flip(value_rows, 0), log_decay[1]
    )
    combined = forward + jnp.flip(backward, 0)
    average = jnp.mean(combined, axis=-1, keepdims=True)
    centred = combined - average
    variance = jnp.mean(centred * centred, axis=-1, keepdims=True)
    return (centred * lax.rsqrt(variance + 1e-06)).astype(jnp.bfloat16)


def shards(tokens, query_weight, key_weight, value_weight, output_weight, log_decay):
    rows = tokens[0]
    row_count = rows.shape[0]
    local_heads = log_decay.shape[1]
    first_head = lax.axis_index("sp") * local_heads
    own_slices = jnp.concatenate(
        [
            lax.dynamic_slice_in_dim(query_weight, first_head * DK, local_heads * DK, 1),
            lax.dynamic_slice_in_dim(key_weight, first_head * DK, local_heads * DK, 1),
            lax.dynamic_slice_in_dim(value_weight, first_head * DV, local_heads * DV, 1),
        ],
        axis=1,
    )
    own_whole = lax.all_gather(own_slices, "dp", axis=0, tiled=True)
    piece = lax.all_gather(rows, "sp", axis=0, tiled=True)
    count = piece.shape[0]
    product = jnp.dot(piece, own_whole, preferred_element_type=jnp.float32).astype(jnp.bfloat16)
    query_part = product[:, : local_heads * DK].reshape(count, local_heads, DK)
    key_part = product[:, local_heads * DK : 2 * local_heads * DK].reshape(count, local_heads, DK)
    value_part = product[:, 2 * local_heads * DK :].reshape(count, local_heads, DV)
    gathered = jnp.concatenate([query_part, key_part, value_part], axis=2)
    normed = mechanism(gathered, log_decay)
    by_token = lax.all_to_all(normed, "sp", split_axis=0, concat_axis=1, tiled=True).reshape(
        row_count, HEADS * DV
    )
    mixed = jnp.dot(
        by_token,
        lax.all_gather(output_weight, "dp", axis=0, tiled=True),
        preferred_element_type=jnp.float32,
    )
    return mixed.astype(jnp.bfloat16)[None]


MESH = pl.DeviceIdType.MESH
CORES = 2
PIECES = 2


def tables(length):
    half = DK // 2
    frequency = (10000.0 ** (-np.arange(half) / half)).astype(np.float32)
    angles = (np.arange(length, dtype=np.float32)[:, None] * frequency[None, :]).astype(np.float64)
    cosine = np.tile(np.cos(angles), (1, 4)).astype(np.float32)
    sine = np.tile(np.sin(angles), (1, 4)).astype(np.float32)
    swap = np.zeros((2 * DK, 2 * DK), np.float32)
    for lane in range(2 * DK):
        if lane % DK < half:
            swap[lane + half, lane] = -1.0
        else:
            swap[lane - half, lane] = 1.0
    return jnp.asarray(cosine), jnp.asarray(sine), jnp.asarray(swap, jnp.bfloat16)


def layer_kernel(
    S, Z, rate_ref, cos_ref, sin_ref, swap_ref, x_ref, wq_ref, wk_ref, wv_ref, wo_ref, out_ref,
    tok, wqkv, wo, acc, decay, qk, val, nsend, nrm, oacc,
    lsem, tS, tR, qS, qR, qpS, qpR, oS, oR, iS, iR, dS, dR, opS, opR, nS, nR,
):
    s = lax.axis_index("sp")
    d = lax.axis_index("dp")
    z, c = d // CORES, d % CORES
    rows, model = x_ref.shape
    length = S * rows
    depth = wq_ref.shape[0]
    heads = rate_ref.shape[1]
    qc, vc = heads * DK, heads * DV
    oc = wo.shape[3]
    step_rows = depth // PIECES
    sx = s + 1 - 2 * (s % 2)
    sy = (s + 2) % 4
    sd = (sx + 2) % 4
    partner = {"dp": z * CORES + 1 - c}

    def remote(src, send, recv, device, dst=None):
        return pltpu.make_async_remote_copy(
            src_ref=src, dst_ref=src if dst is None else dst, send_sem=send, recv_sem=recv,
            device_id=device, device_id_type=MESH,
        )

    local = [
        pltpu.make_async_copy(wq_ref.at[:, pl.ds(pl.multiple_of(s * qc, qc), qc)], wqkv.at[d, :, pl.ds(0, qc)], lsem.at[0]),
        pltpu.make_async_copy(wk_ref.at[:, pl.ds(pl.multiple_of(s * qc, qc), qc)], wqkv.at[d, :, pl.ds(qc, qc)], lsem.at[1]),
        pltpu.make_async_copy(wv_ref.at[:, pl.ds(pl.multiple_of(s * vc, vc), vc)], wqkv.at[d, :, pl.ds(2 * qc, vc)], lsem.at[2]),
        pltpu.make_async_copy(x_ref, tok.at[s], lsem.at[3]),
    ] + [
        pltpu.make_async_copy(wo_ref.at[:, pl.ds(j * oc, oc)], wo.at[d, j], lsem.at[4 + j]) for j in range(S)
    ]
    for copy in local:
        copy.start()

    barrier = pltpu.get_barrier_semaphore()

    def greet(device):
        pl.semaphore_signal(barrier, inc=1, device_id=device, device_id_type=MESH)

    for other in range(1, S):
        greet({"sp": (s + other) % S})
    greet(partner)
    pl.when(z > 0)(lambda: greet({"dp": d - CORES}))
    pl.when(z < Z - 1)(lambda: greet({"dp": d + CORES}))
    inside = (z > 0) & (z < Z - 1)
    pl.when(inside)(lambda: pl.semaphore_wait(barrier, S + 2))
    pl.when(jnp.logical_not(inside))(lambda: pl.semaphore_wait(barrier, S + min(Z - 1, 1)))

    def side(way):
        return {"dp": d + CORES if way == 0 else d - CORES}

    def has_side(way):
        return z < Z - 1 if way == 0 else z > 0

    def q_copy(way, src, piece, to=None):
        ref = wqkv.at[src * CORES + c, pl.ds(piece * step_rows, step_rows)]
        return remote(ref, qS.at[way, src, piece], qR.at[src, piece], side(way if to is None else to))

    def o_piece(block, quarter, piece):
        return wo.at[block, quarter, pl.ds(piece * step_rows, step_rows)]

    def o_copy(way, src, piece, to=None):
        return remote(o_piece(src * CORES + c, s, piece), oS.at[way, src, piece], oR.at[src, piece], side(way if to is None else to))

    def qp_copy(src, mine=True):
        ref = wqkv.at[src * CORES + (c if mine else 1 - c)]
        return remote(ref, qpS.at[src], qpR.at[src], partner)

    def op_copy(src, mine=True):
        ref = wo.at[src * CORES + (c if mine else 1 - c)]
        return remote(ref, opS.at[src], opR.at[src], partner)

    def i_copy(axis, src, piece, mine=True):
        to = sx if axis == 0 else sy
        return remote(o_piece(src * CORES + c, s if mine else to, piece), iS.at[axis, src, piece], iR.at[axis, src, piece], {"sp": to})

    def d_copy(src, piece, mine=True):
        first = piece < PIECES // 2
        to = sy if first else sx
        quarter = (sx if first else sy) if mine else sd
        return remote(o_piece(src * CORES + c, quarter, piece), dS.at[src, piece], dR.at[src, piece], {"sp": to})

    def t_copy(other):
        to = (s + other) % S
        return remote(tok.at[s], tS.at[other], tR.at[other], {"sp": to})

    def t_wait(other):
        frm = (s + S - other) % S
        remote(tok.at[frm], tS.at[other], tR.at[other], {"sp": frm}).wait_recv()

    def n_copy(head, j):
        return remote(
            nsend.at[head, j], nS.at[head, j], nR.at[head, s], {"sp": j},
            dst=nrm.at[s, :, pl.ds(head * DV, DV)],
        )

    def n_wait(head, j):
        remote(nsend.at[head, j], nS.at[head, j], nR.at[head, j], {"sp": j}, dst=nrm.at[j, :, pl.ds(head * DV, DV)]).wait_recv()

    def each(count, fn):
        for piece in range(count):
            fn(piece)

    def own_o(way):
        each(PIECES, lambda piece: o_copy(way, z, piece).start())

    for copy in local[:3]:
        copy.wait()
    for way in (0, 1):
        pl.when(has_side(way))(lambda way=way: each(PIECES, lambda piece: q_copy(way, z, piece).start()))
    local[3].wait()
    for other in range(1, S):
        t_copy(other).start()
    qp_copy(z).start()
    for copy in local[4:]:
        copy.wait()
    for way in (0, 1):
        pl.when(has_side(way))(lambda way=way: own_o(way))
    op_copy(z).start()

    for head in range(heads):
        fast, slow = rate_ref[0, head], rate_ref[1, head]

        @pl.loop(0, S)
        def _(j):
            at = lax.broadcasted_iota(jnp.int32, (rows, length), 0) + j * rows
            gap = (at - lax.broadcasted_iota(jnp.int32, (rows, length), 1)).astype(jnp.float32)
            weight = jnp.exp(jnp.where(gap >= 0.0, gap * fast, gap * (-slow)))
            decay[head, pl.ds(pl.multiple_of(j * rows, rows), rows), :] = jnp.where(gap == 0.0, 2.0, weight)

    width = 2 * qc + vc
    tile = 256

    def project(src, first):
        qp_copy(src, mine=False).wait_recv()
        wide = CORES * depth
        cols = pl.ds(pl.multiple_of(src * wide, wide), wide)

        @pl.loop(0, width // tile)
        def _(n):
            at = pl.ds(pl.multiple_of(n * tile, tile), tile)
            part = jnp.dot(
                tok[:, :, cols].reshape(length, wide),
                wqkv[pl.ds(src * CORES, CORES), :, at].reshape(wide, tile),
                preferred_element_type=jnp.float32,
            )
            if first:
                acc[:, at] = part
            else:
                acc[:, at] += part

    def sources(k):
        return ((0, z - k, z - k >= 0), (1, z + k, z + k < Z))

    def q_step(k):
        for way, src, there in sources(k):
            @pl.when(there)
            def _():
                for piece in range(PIECES):
                    q_copy(way, src, piece, 1 - way).wait_recv()
                    pl.when(has_side(way))(lambda: q_copy(way, src, piece).start())
                qp_copy(src).start()

    def o_step(k):
        for way, src, there in sources(k):
            @pl.when(there)
            def _():
                for piece in range(PIECES):
                    o_copy(way, src, piece, 1 - way).wait_recv()
                    pl.when(has_side(way))(lambda: o_copy(way, src, piece).start())
                for piece in range(PIECES):
                    i_copy(0, src, piece).start()
                    i_copy(1, src, PIECES - 1 - piece).start()

    def o_relay(k):
        for way, src, there in sources(k):
            @pl.when(there)
            def _():
                for near in range(PIECES // 2):
                    for axis, piece in ((0, near), (1, PIECES - 1 - near)):
                        i_copy(axis, src, piece, mine=False).wait_recv()
                        d_copy(src, piece).start()

    def o_share(k):
        for way, src, there in sources(k):
            @pl.when(there)
            def _():
                for near in range(PIECES // 2):
                    i_copy(1, src, near, mine=False).wait_recv()
                    i_copy(0, src, PIECES - 1 - near, mine=False).wait_recv()
                for piece in range(PIECES):
                    d_copy(src, piece, mine=False).wait_recv()
                op_copy(src).start()

    def project_step(k):
        for way, src, there in sources(k):
            pl.when(there)(lambda: project(src, False))

    q_step(1)
    o_step(1)
    for other in range(1, S):
        t_wait(other)
    project(z, True)
    project_step(1)
    q_step(2)
    o_step(2)
    o_relay(1)
    project_step(2)
    q_step(3)
    project_step(3)

    for pair in range(qc // (2 * DK)):
        for part in range(2):
            at = pl.ds(part * qc + pair * 2 * DK, 2 * DK)
            flat = acc[:, at].astype(jnp.bfloat16)
            turned = jnp.dot(flat, swap_ref[...], preferred_element_type=jnp.float32)
            qk[:, at] = (flat.astype(jnp.float32) * cos_ref[...] + turned * sin_ref[...]).astype(jnp.bfloat16)
    val[...] = acc[:, 2 * qc :].astype(jnp.bfloat16)

    def retain_head(head):
        pair = head // 2
        lane = lax.broadcasted_iota(jnp.int32, (rows, 2 * DK), 1)
        mine = (lane // DK) == (head % 2)
        for j in range(S):
            here = slice(j * rows, (j + 1) * rows)
            query = qk[here, pair * 2 * DK : (pair + 1) * 2 * DK]
            query = jnp.where(mine, query.astype(jnp.float32), 0.0).astype(jnp.bfloat16)
            scores = lax.dot_general(
                query, qk[:, qc + pair * 2 * DK : qc + (pair + 1) * 2 * DK],
                (((1,), (1,)), ((), ())), preferred_element_type=jnp.float32,
            )
            scores = (scores * decay[head, here, :]).astype(jnp.bfloat16)
            ret = jnp.dot(scores, val[:, head * DV : (head + 1) * DV], preferred_element_type=jnp.float32)
            centred = ret - jnp.mean(ret, axis=-1, keepdims=True)
            variance = jnp.mean(centred * centred, axis=-1, keepdims=True)
            normed = (centred * lax.rsqrt(variance + 1e-06)).astype(jnp.bfloat16)
            nsend[head, j] = normed

            @pl.when(j == s)
            def _():
                nrm[s, :, head * DV : (head + 1) * DV] = normed

            @pl.when(j != s)
            def _():
                n_copy(head, j).start()

    def finish(src, first):
        op_copy(src, mine=False).wait_recv()

        @pl.loop(0, S)
        def _(j):
            at = pl.ds(pl.multiple_of(j * oc, oc), oc)
            part = jnp.dot(
                nrm[src], wo[pl.ds(src * CORES, CORES), j].reshape(CORES * depth, oc),
                preferred_element_type=jnp.float32,
            )
            if first:
                oacc[:, at] = part
            else:
                oacc[:, at] += part

    def finish_step(k):
        for way, src, there in sources(k):
            pl.when(there)(lambda: finish(src, False))

    for head in range(heads):
        retain_head(head)
        if head == 0:
            o_relay(2)
        if head == heads - 2:
            o_step(3)
    o_share(1)
    o_relay(3)
    for j in range(S):
        @pl.when(j != s)
        def _():
            for head in range(heads):
                n_wait(head, j)
    finish(z, True)
    finish_step(1)
    o_share(2)
    o_share(3)
    finish_step(2)
    finish_step(3)
    out_ref[...] = oacc[...].astype(out_ref.dtype)

    for other in range(1, S):
        t_copy(other).wait_send()
    for way in (0, 1):
        @pl.when(has_side(way))
        def _():
            for piece in range(PIECES):
                q_copy(way, z, piece).wait_send()
                o_copy(way, z, piece).wait_send()
    qp_copy(z).wait_send()
    op_copy(z).wait_send()
    for k in range(1, Z):
        for way, src, there in sources(k):
            @pl.when(there)
            def _():
                qp_copy(src).wait_send()
                op_copy(src).wait_send()
                for piece in range(PIECES):
                    i_copy(0, src, piece).wait_send()
                    i_copy(1, src, piece).wait_send()
                    d_copy(src, piece).wait_send()

            @pl.when(there & has_side(way))
            def _():
                for piece in range(PIECES):
                    q_copy(way, src, piece).wait_send()
                    o_copy(way, src, piece).wait_send()
    for head in range(heads):
        for j in range(S):
            pl.when(j != s)(lambda: n_copy(head, j).wait_send())


def fused(S, Z, tokens, query_weight, key_weight, value_weight, output_weight, log_decay):
    rows, model = tokens.shape[1:]
    depth = query_weight.shape[0]
    heads = log_decay.shape[1]
    length = S * rows
    width = heads * (2 * DK + DV)
    oc = output_weight.shape[1] // S
    cosine, sine, swap = tables(length)
    vmem, anyplace = pl.BlockSpec(memory_space=pltpu.VMEM), pl.BlockSpec(memory_space=pl.ANY)
    dma = pltpu.SemaphoreType.DMA
    bf, f32 = jnp.bfloat16, jnp.float32
    out = pl.pallas_call(
        functools.partial(layer_kernel, S, Z),
        out_shape=jax.ShapeDtypeStruct((rows, output_weight.shape[1]), bf),
        in_specs=[pl.BlockSpec(memory_space=pltpu.SMEM)] + [vmem] * 3 + [anyplace] * 5,
        out_specs=vmem,
        scratch_shapes=[
            pltpu.VMEM((S, rows, model), bf),
            pltpu.VMEM((Z * CORES, depth, width), bf),
            pltpu.VMEM((Z * CORES, S, depth, oc), bf),
            pltpu.VMEM((length, width), f32),
            pltpu.VMEM((heads, length, length), f32),
            pltpu.VMEM((length, 2 * heads * DK), bf),
            pltpu.VMEM((length, heads * DV), bf),
            pltpu.VMEM((heads, S, rows, DV), bf),
            pltpu.VMEM((S, rows, heads * DV), bf),
            pltpu.VMEM((rows, S * oc), f32),
            dma((4 + S,)), dma((S,)), dma((S,)),
            dma((2, Z, PIECES)), dma((Z, PIECES)), dma((Z,)), dma((Z,)),
            dma((2, Z, PIECES)), dma((Z, PIECES)),
            dma((2, Z, PIECES)), dma((2, Z, PIECES)), dma((Z, PIECES)), dma((Z, PIECES)),
            dma((Z,)), dma((Z,)), dma((heads, S)), dma((heads, S)),
        ],
        compiler_params=pltpu.CompilerParams(
            collective_id=0, has_side_effects=True, vmem_limit_bytes=60 * 1024 * 1024
        ),
    )(log_decay, cosine, sine, swap, tokens[0], query_weight, key_weight, value_weight, output_weight)
    return out[None]


def solution(mesh):
    S, D = mesh.shape["sp"], mesh.shape["dp"]
    Z = D // CORES

    def layer(tokens, query_weight, key_weight, value_weight, output_weight, log_decay):
        rows = tokens.shape[1]
        depth = query_weight.shape[0]
        heads = log_decay.shape[1]
        fits = (
            S == 4 and D == CORES * Z and S * rows == BLOCK and (heads * DK) % 256 == 0
            and heads * DV == CORES * depth and rows % 128 == 0
        )
        args = (tokens, query_weight, key_weight, value_weight, output_weight, log_decay)
        return fused(S, Z, *args) if fits else shards(*args)

    placed = (
        P("dp", "sp", None),
        P("dp", None),
        P("dp", None),
        P("dp", None),
        P("dp", None),
        P(None, "sp"),
    )
    return jax.shard_map(
        layer, mesh=mesh, in_specs=placed, out_specs=P("dp", "sp", None), check_vma=False
    )
```

profile of v0, /device:TPU:0, one launch (start us, length us, event | category | flops | bytes accessed | tf_op | source)
XLA Modules:
  0.0 83.7 jit_solution(9006753730702439923)
XLA Ops:
  0.0 81.8 %shard_map.91 = bf16[128,2048]{1,0:T(8,128)(2,1)} custom-call(f32[2,4]{1,0:T(2,128)} %rate_ref.1, f32[512,128]{1,0:T(8,128)} %constant.6.clone.cos_ref, f32[512,128]{1,0:T(8,128)} %constant.7.clone.sin_ref, bf16[128,128]{1,0:T(8,128)(2,1)} %constant.8.clone.swap_ref, bf16[128,2048]{1,0:T(8,128)(2,1)} %bitcast.3, bf16[256,1024]{1,0:T(8,128)(2,1)} %wq_ref.1, ...), custom_call_target="tpu_custom_call" | custom-call | tf_op jit(solution)/shard_map/pallas_call | solution.py:480
  81.8 1.9 %copy.11 = bf16[1,128,2048]{2,1,0:T(8,128)(2,1)} copy(bf16[1,128,2048]{2,1,0:T(8,128)(2,1)} %bitcast.2) | data formatting | bytes 1048576
where the time goes:
time: 83.8 us; the launch traced here: 83.7 us
  Pallas kernels  81.8 us (98%)
  local copies, waits for them, and re-layouts  1.88 us (2%)
    pallas_call x1, Pallas kernels, fused(): pl.pallas_call(functools.partial(layer_kernel, S, Z), out_shape=jax.Shape...  81.8 us
    unnamed x1, local copies, waits for them, and re-layouts  1.88 us

commit v1 on v0

v1 whole, which is shorter than its diff:
```python
import functools

import numpy as np
import jax
import jax.numpy as jnp
from jax import lax
from jax.experimental import pallas as pl
from jax.experimental.pallas import tpu as pltpu
from jax.sharding import PartitionSpec as P

HEADS = 16
DK = 64
DV = 128
BLOCK = 512


exact_precision = lax.Precision.HIGHEST


def rotate(values_part, positions):
    half_dim = values_part.shape[-1] // 2
    frequency = 10000.0 ** (-jnp.arange(half_dim, dtype=jnp.float32) / half_dim)
    angles = positions[:, None] * frequency[None, :]
    cosine = jnp.cos(angles)[:, None, :]
    sine_part = jnp.sin(angles)[:, None, :]
    first = values_part[..., :half_dim]
    second = values_part[..., half_dim:]
    return jnp.concatenate(
        [first * cosine - second * sine_part, first * sine_part + second * cosine], axis=-1
    )


def retain(query, key_rows, value_rows, log_rate):
    length, heads, key_dim = query.shape
    value_dim = value_rows.shape[-1]
    count = length // BLOCK
    offsets = jnp.arange(BLOCK, dtype=jnp.float32)
    distance = offsets[:, None] - offsets[None, :]
    decay_inner = jnp.where(
        distance[None] >= 0.0,
        jnp.exp(log_rate[:, None, None] * jnp.maximum(distance, 0.0)[None]),
        0.0,
    )
    decay_query = jnp.exp((offsets[:, None] + 1.0) * log_rate[None, :])[:, :, None]
    decay_key = jnp.exp((BLOCK - 1.0 - offsets)[:, None] * log_rate[None, :])[:, :, None]
    decay_block = jnp.exp(BLOCK * log_rate)[:, None, None]

    def blocks(array):
        return array.reshape(count, BLOCK, heads, array.shape[-1])

    def advance(state, inputs):
        query_block, key_block, value_block = inputs
        inner = (
            jnp.einsum("ihd,jhd->hij", query_block, key_block, preferred_element_type=jnp.float32)
            * decay_inner
        )
        result = jnp.einsum(
            "hij,jhv->ihv",
            inner.astype(jnp.bfloat16),
            value_block,
            preferred_element_type=jnp.float32,
        )
        query_wide = query_block.astype(jnp.float32) * decay_query
        result = result + jnp.einsum("ihd,hdv->ihv", query_wide, state, precision=exact_precision)
        key_wide = key_block.astype(jnp.float32) * decay_key
        state = state * decay_block + jnp.einsum(
            "jhd,jhv->hdv", key_wide, value_block.astype(jnp.float32), precision=exact_precision
        )
        return (state, result)

    initial = jnp.zeros((heads, key_dim, value_dim), jnp.float32)
    final_state, outputs = lax.scan(
        advance, initial, (blocks(query), blocks(key_rows), blocks(value_rows))
    )
    return outputs.reshape(length, heads, value_dim)


def mechanism(stacked, log_decay):
    length = stacked.shape[0]
    widened = stacked[..., : 2 * DK].astype(jnp.float32)
    positions = jnp.arange(length, dtype=jnp.float32)
    query = rotate(widened[..., :DK], positions).astype(jnp.bfloat16)
    key_rows = rotate(widened[..., DK : 2 * DK], positions).astype(jnp.bfloat16)
    value_rows = stacked[..., 2 * DK :]
    forward = retain(query, key_rows, value_rows, log_decay[0])
    backward = retain(
        jnp.flip(query, 0), jnp.flip(key_rows, 0), jnp.flip(value_rows, 0), log_decay[1]
    )
    combined = forward + jnp.flip(backward, 0)
    average = jnp.mean(combined, axis=-1, keepdims=True)
    centred = combined - average
    variance = jnp.mean(centred * centred, axis=-1, keepdims=True)
    return (centred * lax.rsqrt(variance + 1e-06)).astype(jnp.bfloat16)


def shards(tokens, query_weight, key_weight, value_weight, output_weight, log_decay):
    rows = tokens[0]
    row_count = rows.shape[0]
    local_heads = log_decay.shape[1]
    first_head = lax.axis_index("sp") * local_heads
    own_slices = jnp.concatenate(
        [
            lax.dynamic_slice_in_dim(query_weight, first_head * DK, local_heads * DK, 1),
            lax.dynamic_slice_in_dim(key_weight, first_head * DK, local_heads * DK, 1),
            lax.dynamic_slice_in_dim(value_weight, first_head * DV, local_heads * DV, 1),
        ],
        axis=1,
    )
    own_whole = lax.all_gather(own_slices, "dp", axis=0, tiled=True)
    piece = lax.all_gather(rows, "sp", axis=0, tiled=True)
    count = piece.shape[0]
    product = jnp.dot(piece, own_whole, preferred_element_type=jnp.float32).astype(jnp.bfloat16)
    query_part = product[:, : local_heads * DK].reshape(count, local_heads, DK)
    key_part = product[:, local_heads * DK : 2 * local_heads * DK].reshape(count, local_heads, DK)
    value_part = product[:, 2 * local_heads * DK :].reshape(count, local_heads, DV)
    gathered = jnp.concatenate([query_part, key_part, value_part], axis=2)
    normed = mechanism(gathered, log_decay)
    by_token = lax.all_to_all(normed, "sp", split_axis=0, concat_axis=1, tiled=True).reshape(
        row_count, HEADS * DV
    )
    mixed = jnp.dot(
        by_token,
        lax.all_gather(output_weight, "dp", axis=0, tiled=True),
        preferred_element_type=jnp.float32,
    )
    return mixed.astype(jnp.bfloat16)[None]


MESH = pl.DeviceIdType.MESH
CORES = 2
PAIR = 2
PIECES = 2
LANES = PAIR * DK


def tables(length):
    half = DK // 2
    frequency = (10000.0 ** (-np.arange(half) / half)).astype(np.float32)
    angles = (np.arange(length, dtype=np.float32)[:, None] * frequency[None, :]).astype(np.float64)
    cosine = np.tile(np.cos(angles), (1, 4)).astype(np.float32)
    sine = np.tile(np.sin(angles), (1, 4)).astype(np.float32)
    swap = np.zeros((LANES, LANES), np.float32)
    for lane in range(LANES):
        if lane % DK < half:
            swap[lane + half, lane] = -1.0
        else:
            swap[lane - half, lane] = 1.0
    return jnp.asarray(cosine), jnp.asarray(sine), jnp.asarray(swap, jnp.bfloat16)


def layer_kernel(
    S, Z, rate_hbm, cos_hbm, sin_hbm, swap_hbm, x_ref, wq_ref, wk_ref, wv_ref, wo_ref, out_ref,
    tok, wqkv, wo, acc, decay, qk, val, sc, nown, nrm, oacc, cos_ref, sin_ref, swap_ref, rate_ref,
    lsem, send, tR, rR, qR, qpR, oR, iR, jR, dR, opR, nR,
):
    s = lax.axis_index("sp")
    d = lax.axis_index("dp")
    z, c = d // CORES, d % CORES
    rows, model = x_ref.shape
    length = S * rows
    depth = wq_ref.shape[0]
    heads = rate_hbm.shape[1]
    groups = heads // PAIR
    qc, vc = heads * DK, heads * DV
    wide_v = PAIR * DV
    width = 2 * LANES + wide_v
    oc = wo.shape[3]
    step_rows = depth // PIECES
    half_model = model // 2
    sx = s + 1 - 2 * (s % 2)
    sy = (s + 2) % 4
    sd = (sx + 2) % 4
    partner = {"dp": z * CORES + 1 - c}
    end = (z == 0) | (z == Z - 1)
    mid = jnp.logical_not(end)

    near, across, mirror = z + 1 - 2 * (z % 2), (z + 2) % Z, Z - 1 - z
    second = jnp.where(end, across, mirror)
    third = jnp.where(end, mirror, across)
    o_first = jnp.where(end, near, mirror)
    o_second = jnp.where(end, across, near)

    def remote(src, send_at, recv, device, dst=None):
        return pltpu.make_async_remote_copy(
            src_ref=src, dst_ref=src if dst is None else dst, send_sem=send.at[send_at], recv_sem=recv,
            device_id=device, device_id_type=MESH,
        )

    def local(src, dst, at):
        return pltpu.make_async_copy(src, dst, lsem.at[at])

    def weight_copies(group):
        def part(ref, at, size, to):
            cols = pl.ds(pl.multiple_of(at + group * size, size), size)
            return local(ref.at[:, cols], wqkv.at[d, group, :, pl.ds(to, size)], group)

        return [
            part(wq_ref, s * qc, LANES, 0), part(wk_ref, s * qc, LANES, LANES),
            part(wv_ref, s * vc, wide_v, 2 * LANES),
        ]

    def quarter_copy(j):
        at = (s + j) % S
        return local(wo_ref.at[:, pl.ds(pl.multiple_of(at * oc, oc), oc)], wo.at[d, at], 3 if j == 0 else 4)

    def local_wait(ref, at):
        local(ref, ref, at).wait()

    local_c = [
        local(rate_hbm, rate_ref, 5), local(cos_hbm, cos_ref, 6),
        local(sin_hbm, sin_ref, 7), local(swap_hbm, swap_ref, 8),
    ]
    for copy in (
        weight_copies(0) + [local(x_ref, tok.at[s], 2), quarter_copy(0)] + weight_copies(1)
        + local_c[:1] + [quarter_copy(j) for j in range(1, S)] + local_c[1:]
    ):
        copy.start()

    barrier = pltpu.get_barrier_semaphore()

    def greet(device):
        pl.semaphore_signal(barrier, inc=1, device_id=device, device_id_type=MESH)

    pl.when(z > 0)(lambda: greet({"dp": d - CORES}))
    pl.when(z < Z - 1)(lambda: greet({"dp": d + CORES}))
    for other in range(1, S):
        greet({"sp": (s + other) % S})
    greet(partner)
    pl.when(mid)(lambda: pl.semaphore_wait(barrier, S + 2))
    pl.when(end)(lambda: pl.semaphore_wait(barrier, S + 1))

    def side(way):
        return {"dp": d + CORES - 2 * CORES * way}

    def way_of(src):
        return jnp.where(src < z, 0, 1)

    def q_ref(block, item):
        if item == 0:
            return wqkv.at[block, 0]
        return wqkv.at[block, 1, :, pl.ds((item - 1) * 2 * LANES, 2 * LANES)]

    def q_copy(way, src, item):
        return remote(q_ref(src * CORES + c, item), 0, qR.at[src, item], side(way))

    def qp_copy(src, item, mine=True):
        return remote(q_ref(src * CORES + (c if mine else 1 - c), item), 2, qpR.at[src, item], partner)

    def o_piece(block, quarter, piece):
        return wo.at[block, quarter, pl.ds(piece * step_rows, step_rows)]

    def o_copy(way, src, piece):
        return remote(o_piece(src * CORES + c, s, piece), 1, oR.at[src, piece], side(way))

    def op_copy(src, quarter):
        return remote(wo.at[src * CORES + c, quarter], 3, opR.at[src], partner)

    def i_copy(axis, src, piece, mine=True):
        to = sx if axis == 0 else sy
        recv = iR.at[axis, src] if axis == piece else jR.at[src]
        return remote(o_piece(src * CORES + c, s if mine else to, piece), 4, recv, {"sp": to})

    def d_copy(src, piece):
        to, quarter = (sy, sx) if piece == 0 else (sx, sy)
        return remote(o_piece(src * CORES + c, quarter, piece), 5, dR.at[src], {"sp": to})

    def t_ref(block, half):
        return tok.at[block, :, pl.ds(half * half_model, half_model)]

    def t_copy(axis, half, mine=True):
        to = sx if axis == 0 else sy
        return remote(t_ref(s if mine else to, half), 6, tR.at[axis, half], {"sp": to})

    def r_copy(half, mine=True):
        to, block = (sy, sx) if half == 0 else (sx, sy)
        return remote(t_ref(block if mine else sd, half), 6, rR.at[half], {"sp": to})

    def n_copy(head, to):
        return remote(
            nown.at[head, pl.ds(pl.multiple_of(to * rows, rows), rows)], 7, nR.at[head // PAIR, s], {"sp": to},
            dst=nrm.at[s, :, pl.ds(head * DV, DV)],
        )

    def n_wait(group, j):
        ref = nrm.at[j, :, pl.ds(group * wide_v, wide_v)]
        remote(ref, 7, nR.at[group, j], {"sp": j}).wait_recv()

    def ways(fn):
        for way in (0, 1):
            pl.when(z < Z - 1 if way == 0 else z > 0)(functools.partial(fn, way))

    def start_all(copies):
        for copy in copies:
            copy.start()

    def own_q(items):
        ways(lambda way: start_all([q_copy(way, z, item) for item in items]))

    def own_o():
        ways(lambda way: start_all([o_copy(way, z, piece) for piece in range(PIECES)]))

    local_wait(wqkv.at[d, 0], 0)
    own_q((0,))
    local_wait(tok.at[s], 2)
    for half in range(2):
        t_copy(0, half).start()
        t_copy(1, 1 - half).start()
    qp_copy(z, 0).start()
    local_wait(wo.at[d, s], 3)
    own_o()
    local_wait(wqkv.at[d, 1], 1)
    pl.when(end)(lambda: own_q((1, 2)))
    qp_copy(z, 1).start()
    qp_copy(z, 2).start()

    def decays(group):
        for head in range(group * PAIR, (group + 1) * PAIR):
            fast, slow = rate_ref[0, head], rate_ref[1, head]

            @pl.loop(0, S)
            def _(j):
                at = lax.broadcasted_iota(jnp.int32, (rows, length), 0) + j * rows
                gap = (at - lax.broadcasted_iota(jnp.int32, (rows, length), 1)).astype(jnp.float32)
                weight = jnp.exp(jnp.where(gap >= 0.0, gap * fast, gap * (-slow)))
                decay[head, pl.ds(pl.multiple_of(j * rows, rows), rows), :] = jnp.where(gap == 0.0, 2.0, weight)

    def q_step(src, items):
        way = way_of(src)
        onward = jnp.where(src < z, z < Z - 1, z > 0)
        for item in items:
            q_copy(1 - way, src, item).wait_recv()
            pl.when(onward)(lambda: q_copy(way, src, item).start())
            qp_copy(src, item).start()

    def o_step(src):
        way = way_of(src)
        onward = jnp.where(src < z, z < Z - 1, z > 0)
        for piece in range(PIECES):
            o_copy(1 - way, src, piece).wait_recv()
            pl.when(onward)(lambda: o_copy(way, src, piece).start())
            i_copy(piece, src, piece).start()
            i_copy(1 - piece, src, piece).start()
        op_copy(src, s).start()

    def o_relay(src):
        for piece in range(PIECES):
            i_copy(piece, src, piece, mine=False).wait_recv()
            d_copy(src, piece).start()

    def o_share(src):
        remote(wo.at[src * CORES + c, sx], 4, jR.at[src], {"sp": sx}).wait_recv()
        op_copy(src, sx).start()
        op_copy(src, sy).start()
        remote(wo.at[src * CORES + c, sd], 5, dR.at[src], {"sp": sx}).wait_recv()
        op_copy(src, sd).start()

    def o_ready(src):
        remote(wo.at[src * CORES + 1 - c], 3, opR.at[src], partner).wait_recv()

    tile = 2 * LANES

    def project(src, group, parts, first=False):
        wide = CORES * depth
        cols = pl.ds(pl.multiple_of(src * wide, wide), wide)
        for n in parts:
            at = slice(n * tile, (n + 1) * tile)
            part = jnp.dot(
                tok[:, :, cols].reshape(length, wide),
                wqkv[pl.ds(src * CORES, CORES), group, :, at].reshape(wide, tile),
                preferred_element_type=jnp.float32,
            )
            if first:
                acc[group, :, at] = part
            else:
                acc[group, :, at] += part

    def project_a(src, first=False):
        qp_copy(src, 0, mine=False).wait_recv()
        project(src, 0, (0, 1), first)

    def project_b(src, first=False, parts=(0, 1)):
        for n in parts:
            qp_copy(src, 1 + n, mine=False).wait_recv()
        project(src, 1, parts, first)

    def scores(group):
        for part in range(2):
            at = slice(part * LANES, (part + 1) * LANES)
            flat = acc[group, :, at].astype(jnp.bfloat16)
            turned = jnp.dot(flat, swap_ref[...], preferred_element_type=jnp.float32)
            qk[group, :, at] = (flat.astype(jnp.float32) * cos_ref[...] + turned * sin_ref[...]).astype(jnp.bfloat16)
        lane = lax.broadcasted_iota(jnp.int32, (length, LANES), 1)
        for inner in range(PAIR):
            query = qk[group, :, :LANES]
            query = jnp.where((lane // DK) == inner, query.astype(jnp.float32), 0.0).astype(jnp.bfloat16)
            for n in range(length // tile):
                at = slice(n * tile, (n + 1) * tile)
                part = lax.dot_general(
                    query, qk[group, at, LANES:], (((1,), (1,)), ((), ())), preferred_element_type=jnp.float32,
                )
                sc[inner, :, at] = (part * decay[group * PAIR + inner, :, at]).astype(jnp.bfloat16)

    def values(group):
        val[group] = acc[group, :, 2 * LANES :].astype(jnp.bfloat16)
        for inner in range(PAIR):
            head = group * PAIR + inner
            ret = jnp.dot(sc[inner], val[group, :, inner * DV : (inner + 1) * DV], preferred_element_type=jnp.float32)
            centred = ret - jnp.mean(ret, axis=-1, keepdims=True)
            variance = jnp.mean(centred * centred, axis=-1, keepdims=True)
            nown[head] = (centred * lax.rsqrt(variance + 1e-06)).astype(jnp.bfloat16)
            for to in (sd, sx, sy):
                n_copy(head, to).start()
            nrm[s, :, head * DV : (head + 1) * DV] = nown[head, pl.ds(pl.multiple_of(s * rows, rows), rows), :]

    def finish(units, first=False, last=False):
        for src, group in units:
            pl.when(src != s)(lambda: n_wait(group, src))
        for j in range(S):
            at = slice(j * oc, (j + 1) * oc)
            total = None if first else oacc[:, at]
            for src, group in units:
                part = jnp.dot(
                    nrm[src, :, group * wide_v : (group + 1) * wide_v], wo[src * CORES + group, j],
                    preferred_element_type=jnp.float32,
                )
                total = part if total is None else total + part
            if last:
                out_ref[:, at] = total.astype(out_ref.dtype)
            else:
                oacc[:, at] = total

    def on(where, fn, *args):
        pl.when(where)(lambda: fn(*args))

    both = (1, 2)
    local_wait(wo.at[pl.ds(0, S - 1), 0], 4)
    for j in range(S):
        op_copy(z, (s + j) % S).start()
    local_c[0].wait()
    decays(0)
    for half in range(2):
        t_copy(half, half, mine=False).wait_recv()
        r_copy(half).start()
    q_step(near, (0,))
    on(mid, q_step, second, (0,))
    o_step(o_first)
    on(mid, own_q, both)
    on(mid, q_step, near, both)
    for copy in local_c[1:]:
        copy.wait()
    t_copy(0, 1, mine=False).wait_recv()
    t_copy(1, 0, mine=False).wait_recv()
    for half in range(2):
        r_copy(half, mine=False).wait_recv()
    project_a(z, True)
    project_a(near)
    on(end, q_step, second, (0,))
    project_a(second)
    o_step(o_second)
    o_relay(o_first)
    on(end, q_step, near, both)
    q_step(third, (0,))
    on(mid, q_step, second, both)
    project_a(third)
    scores(0)
    values(0)
    decays(1)
    o_share(o_first)
    o_relay(o_second)
    on(mid, o_step, third)
    project_b(z, True)
    project_b(near)
    on(end, q_step, second, both)
    project_b(second)
    o_ready(z)
    o_ready(o_first)
    finish(((z, 0), (o_first, 0)), first=True)
    o_share(o_second)
    on(end, o_step, third)
    o_ready(o_second)
    finish(((o_second, 0),))
    o_relay(third)
    q_step(third, (1,))
    project_b(third, parts=(0,))
    scores(1)
    q_step(third, (2,))
    project_b(third, parts=(1,))
    values(1)
    o_share(third)
    finish(((z, 1), (o_first, 1), (o_second, 1)))
    o_ready(third)
    finish(((third, 0), (third, 1)), last=True)

    def sent(ref, at):
        remote(ref, at, tR.at[0, 0], partner).wait_send()

    for where, count in ((mid, Z + 1), (end, 1)):
        @pl.when(where)
        def _():
            sent(wqkv.at[pl.ds(0, count)], 0)
            sent(wo.at[pl.ds(0, count), 0], 1)
    sent(wqkv.at[pl.ds(0, Z)], 2)
    sent(wo.at[pl.ds(0, Z)], 3)
    sent(wo.at[pl.ds(0, Z - 1), pl.ds(0, 2)], 4)
    sent(wo.at[pl.ds(0, Z - 1), 0], 5)
    sent(tok.at[pl.ds(0, S - 1)], 6)
    sent(nown.at[:, pl.ds(0, (S - 1) * rows)], 7)


def fused(S, Z, tokens, query_weight, key_weight, value_weight, output_weight, log_decay):
    rows, model = tokens.shape[1:]
    depth = query_weight.shape[0]
    heads = log_decay.shape[1]
    groups = heads // PAIR
    length = S * rows
    width = 2 * LANES + PAIR * DV
    oc = output_weight.shape[1] // S
    cosine, sine, swap = tables(length)
    anyplace = pl.BlockSpec(memory_space=pl.ANY)
    dma = pltpu.SemaphoreType.DMA
    bf, f32 = jnp.bfloat16, jnp.float32
    out = pl.pallas_call(
        functools.partial(layer_kernel, S, Z),
        out_shape=pltpu.VMEM((rows, output_weight.shape[1]), bf),
        in_specs=[anyplace] * 9,
        out_specs=pl.BlockSpec(memory_space=pltpu.VMEM),
        scratch_shapes=[
            pltpu.VMEM((S, rows, model), bf),
            pltpu.VMEM((Z * CORES, groups, depth, width), bf),
            pltpu.VMEM((Z * CORES, S, depth, oc), bf),
            pltpu.VMEM((groups, length, width), f32),
            pltpu.VMEM((heads, length, length), f32),
            pltpu.VMEM((groups, length, 2 * LANES), bf),
            pltpu.VMEM((groups, length, PAIR * DV), bf),
            pltpu.VMEM((PAIR, length, length), bf),
            pltpu.VMEM((heads, length, DV), bf),
            pltpu.VMEM((S, rows, heads * DV), bf),
            pltpu.VMEM((rows, S * oc), f32),
            pltpu.VMEM((length, LANES), f32), pltpu.VMEM((length, LANES), f32), pltpu.VMEM((LANES, LANES), bf),
            pltpu.SMEM((2, heads), f32),
            dma((9,)), dma((8,)), dma((2, 2)), dma((2,)), dma((Z, 3)), dma((Z, 3)),
            dma((Z, PIECES)), dma((2, Z)), dma((Z,)), dma((Z,)), dma((Z,)), dma((groups, S)),
        ],
        compiler_params=pltpu.CompilerParams(
            collective_id=0, has_side_effects=True, vmem_limit_bytes=56 * 1024 * 1024
        ),
    )(log_decay, cosine, sine, swap, tokens[0], query_weight, key_weight, value_weight, output_weight)
    return out[None]


def solution(mesh):
    S, D = mesh.shape["sp"], mesh.shape["dp"]
    Z = D // CORES

    def layer(tokens, query_weight, key_weight, value_weight, output_weight, log_decay):
        rows = tokens.shape[1]
        depth = query_weight.shape[0]
        heads = log_decay.shape[1]
        fits = (
            S == 4 and Z == 4 and D == CORES * Z and S * rows == BLOCK and heads == CORES * PAIR
            and PAIR * DV == depth and rows % 128 == 0
        )
        args = (tokens, query_weight, key_weight, value_weight, output_weight, log_decay)
        return fused(S, Z, *args) if fits else shards(*args)

    placed = (
        P("dp", "sp", None),
        P("dp", None),
        P("dp", None),
        P("dp", None),
        P("dp", None),
        P(None, "sp"),
    )
    return jax.shard_map(
        layer, mesh=mesh, in_specs=placed, out_specs=P("dp", "sp", None), check_vma=False
    )
```

time: 83.8 us -> 69.3 us (0.83)
  Pallas kernels: 81.8 us -> 68.3 us
  local copies, waits for them, and re-layouts: 1.88 us -> 0.8 us
    pallas_call x1, Pallas kernels: 81.8 us -> 68.3 us  [fused(): pl.pallas_call(functools.partial(layer_kernel, S, Z), out_shape=pltpu.VME...]
    unnamed x1, local copies, waits for them, and re-layouts: 1.88 us -> 0.8 us
where the time goes in v1:
time: 69.3 us; the launch traced here: 69.1 us
  Pallas kernels  68.3 us (99%)
  local copies, waits for them, and re-layouts  0.8 us (1%)
    pallas_call x1, Pallas kernels, fused(): pl.pallas_call(functools.partial(layer_kernel, S, Z), out_shape=pltpu.VME...  68.3 us

profile of v1, /device:TPU:0, one launch (start us, length us, event | category | flops | bytes accessed | tf_op | source)
XLA Modules:
  0.0 69.1 jit_solution(548321979635497039)
XLA Ops:
  0.0 68.3 %shard_map.91 = bf16[128,2048]{1,0:T(8,128)(2,1)S(1)} custom-call(f32[2,4]{1,0:T(2,128)} %rate_hbm.1, f32[512,128]{1,0:T(8,128)} %constant.6.clone.cos_hbm, f32[512,128]{1,0:T(8,128)} %constant.7.clone.sin_hbm, bf16[128,128]{1,0:T(8,128)(2,1)} %constant.8.clone.swap_hbm, bf16[128,2048]{1,0:T(8,128)(2,1)} %bitcast.3, bf16[256,1024]{1,0:T(8,128)(2,1)} %wq_ref.1, ...), custom_call_target="tpu_custom_call" | custom-call | tf_op jit(solution)/shard_map/pallas_call | solution.py:522
  68.3 0.8 %copy.11 = bf16[1,128,2048]{2,1,0:T(8,128)(2,1)} copy(bf16[1,128,2048]{2,1,0:T(8,128)(2,1)S(1)} %bitcast.2) | data formatting | bytes 1048576

commit v2 on v1

--- a/solution.py
+++ b/solution.py
@@ -444,8 +444,6 @@
     q_step(near, (0,))
     on(mid, q_step, second, (0,))
     o_step(o_first)
-    on(mid, own_q, both)
-    on(mid, q_step, near, both)
     for copy in local_c[1:]:
         copy.wait()
     t_copy(0, 1, mine=False).wait_recv()
@@ -456,34 +454,39 @@
     project_a(near)
     on(end, q_step, second, (0,))
     project_a(second)
-    o_step(o_second)
+    on(mid, q_step, third, (0,))
+    on(mid, o_step, o_second)
+    on(mid, own_q, both)
     o_relay(o_first)
-    on(end, q_step, near, both)
-    q_step(third, (0,))
-    on(mid, q_step, second, both)
+    on(end, o_step, o_second)
+    on(end, q_step, third, (0,))
+    on(mid, q_step, near, both)
     project_a(third)
     scores(0)
     values(0)
+    on(mid, o_step, third)
     decays(1)
     o_share(o_first)
     o_relay(o_second)
-    on(mid, o_step, third)
+    on(mid, q_step, second, both)
+    on(end, q_step, near, both)
     project_b(z, True)
     project_b(near)
-    on(end, q_step, second, both)
-    project_b(second)
+    on(end, o_step, third)
     o_ready(z)
     o_ready(o_first)
     finish(((z, 0), (o_first, 0)), first=True)
+    on(mid, q_step, third, both)
     o_share(o_second)
-    on(end, o_step, third)
     o_ready(o_second)
     finish(((o_second, 0),))
+    on(end, q_step, second, both)
+    project_b(second)
     o_relay(third)
-    q_step(third, (1,))
+    on(end, q_step, third, (1,))
     project_b(third, parts=(0,))
     scores(1)
-    q_step(third, (2,))
+    on(end, q_step, third, (2,))
     project_b(third, parts=(1,))
     values(1)
     o_share(third)

time: 69.3 us -> 65.8 us (0.949)
  Pallas kernels: 68.3 us -> 64.9 us
    pallas_call x1, Pallas kernels: 68.3 us -> 64.9 us  [fused(): pl.pallas_call(functools.partial(layer_kernel, S, Z), out_shape=pltpu.VME...]
where the time goes in v2:
time: 65.8 us; the launch traced here: 65.7 us
  Pallas kernels  64.9 us (99%)
  local copies, waits for them, and re-layouts  0.8 us (1%)
    pallas_call x1, Pallas kernels, fused(): pl.pallas_call(functools.partial(layer_kernel, S, Z), out_shape=pltpu.VME...  64.9 us

profile of v2, /device:TPU:0, one launch (start us, length us, event | category | flops | bytes accessed | tf_op | source)
XLA Modules:
  0.0 65.7 jit_solution(11729580854240272701)
XLA Ops:
  0.0 64.9 %shard_map.91 = bf16[128,2048]{1,0:T(8,128)(2,1)S(1)} custom-call(f32[2,4]{1,0:T(2,128)} %rate_hbm.1, f32[512,128]{1,0:T(8,128)} %constant.6.clone.cos_hbm, f32[512,128]{1,0:T(8,128)} %constant.7.clone.sin_hbm, bf16[128,128]{1,0:T(8,128)(2,1)} %constant.8.clone.swap_hbm, bf16[128,2048]{1,0:T(8,128)(2,1)} %bitcast.3, bf16[256,1024]{1,0:T(8,128)(2,1)} %wq_ref.1, ...), custom_call_target="tpu_custom_call" | custom-call | tf_op jit(solution)/shard_map/pallas_call | solution.py:525
  64.9 0.8 %copy.11 = bf16[1,128,2048]{2,1,0:T(8,128)(2,1)} copy(bf16[1,128,2048]{2,1,0:T(8,128)(2,1)S(1)} %bitcast.2) | data formatting | bytes 1048576

commit v3 on v1

v3 whole, which is shorter than its diff:
```python
import functools

import numpy as np
import jax
import jax.numpy as jnp
from jax import lax
from jax.experimental import pallas as pl
from jax.experimental.pallas import tpu as pltpu
from jax.sharding import PartitionSpec as P

HEADS = 16
DK = 64
DV = 128
BLOCK = 512


exact_precision = lax.Precision.HIGHEST


def rotate(values_part, positions):
    half_dim = values_part.shape[-1] // 2
    frequency = 10000.0 ** (-jnp.arange(half_dim, dtype=jnp.float32) / half_dim)
    angles = positions[:, None] * frequency[None, :]
    cosine = jnp.cos(angles)[:, None, :]
    sine_part = jnp.sin(angles)[:, None, :]
    first = values_part[..., :half_dim]
    second = values_part[..., half_dim:]
    return jnp.concatenate(
        [first * cosine - second * sine_part, first * sine_part + second * cosine], axis=-1
    )


def retain(query, key_rows, value_rows, log_rate):
    length, heads, key_dim = query.shape
    value_dim = value_rows.shape[-1]
    count = length // BLOCK
    offsets = jnp.arange(BLOCK, dtype=jnp.float32)
    distance = offsets[:, None] - offsets[None, :]
    decay_inner = jnp.where(
        distance[None] >= 0.0,
        jnp.exp(log_rate[:, None, None] * jnp.maximum(distance, 0.0)[None]),
        0.0,
    )
    decay_query = jnp.exp((offsets[:, None] + 1.0) * log_rate[None, :])[:, :, None]
    decay_key = jnp.exp((BLOCK - 1.0 - offsets)[:, None] * log_rate[None, :])[:, :, None]
    decay_block = jnp.exp(BLOCK * log_rate)[:, None, None]

    def blocks(array):
        return array.reshape(count, BLOCK, heads, array.shape[-1])

    def advance(state, inputs):
        query_block, key_block, value_block = inputs
        inner = (
            jnp.einsum("ihd,jhd->hij", query_block, key_block, preferred_element_type=jnp.float32)
            * decay_inner
        )
        result = jnp.einsum(
            "hij,jhv->ihv",
            inner.astype(jnp.bfloat16),
            value_block,
            preferred_element_type=jnp.float32,
        )
        query_wide = query_block.astype(jnp.float32) * decay_query
        result = result + jnp.einsum("ihd,hdv->ihv", query_wide, state, precision=exact_precision)
        key_wide = key_block.astype(jnp.float32) * decay_key
        state = state * decay_block + jnp.einsum(
            "jhd,jhv->hdv", key_wide, value_block.astype(jnp.float32), precision=exact_precision
        )
        return (state, result)

    initial = jnp.zeros((heads, key_dim, value_dim), jnp.float32)
    final_state, outputs = lax.scan(
        advance, initial, (blocks(query), blocks(key_rows), blocks(value_rows))
    )
    return outputs.reshape(length, heads, value_dim)


def mechanism(stacked, log_decay):
    length = stacked.shape[0]
    widened = stacked[..., : 2 * DK].astype(jnp.float32)
    positions = jnp.arange(length, dtype=jnp.float32)
    query = rotate(widened[..., :DK], positions).astype(jnp.bfloat16)
    key_rows = rotate(widened[..., DK : 2 * DK], positions).astype(jnp.bfloat16)
    value_rows = stacked[..., 2 * DK :]
    forward = retain(query, key_rows, value_rows, log_decay[0])
    backward = retain(
        jnp.flip(query, 0), jnp.flip(key_rows, 0), jnp.flip(value_rows, 0), log_decay[1]
    )
    combined = forward + jnp.flip(backward, 0)
    average = jnp.mean(combined, axis=-1, keepdims=True)
    centred = combined - average
    variance = jnp.mean(centred * centred, axis=-1, keepdims=True)
    return (centred * lax.rsqrt(variance + 1e-06)).astype(jnp.bfloat16)


def shards(tokens, query_weight, key_weight, value_weight, output_weight, log_decay):
    rows = tokens[0]
    row_count = rows.shape[0]
    local_heads = log_decay.shape[1]
    first_head = lax.axis_index("sp") * local_heads
    own_slices = jnp.concatenate(
        [
            lax.dynamic_slice_in_dim(query_weight, first_head * DK, local_heads * DK, 1),
            lax.dynamic_slice_in_dim(key_weight, first_head * DK, local_heads * DK, 1),
            lax.dynamic_slice_in_dim(value_weight, first_head * DV, local_heads * DV, 1),
        ],
        axis=1,
    )
    own_whole = lax.all_gather(own_slices, "dp", axis=0, tiled=True)
    piece = lax.all_gather(rows, "sp", axis=0, tiled=True)
    count = piece.shape[0]
    product = jnp.dot(piece, own_whole, preferred_element_type=jnp.float32).astype(jnp.bfloat16)
    query_part = product[:, : local_heads * DK].reshape(count, local_heads, DK)
    key_part = product[:, local_heads * DK : 2 * local_heads * DK].reshape(count, local_heads, DK)
    value_part = product[:, 2 * local_heads * DK :].reshape(count, local_heads, DV)
    gathered = jnp.concatenate([query_part, key_part, value_part], axis=2)
    normed = mechanism(gathered, log_decay)
    by_token = lax.all_to_all(normed, "sp", split_axis=0, concat_axis=1, tiled=True).reshape(
        row_count, HEADS * DV
    )
    mixed = jnp.dot(
        by_token,
        lax.all_gather(output_weight, "dp", axis=0, tiled=True),
        preferred_element_type=jnp.float32,
    )
    return mixed.astype(jnp.bfloat16)[None]


MESH = pl.DeviceIdType.MESH
CORES = 2
PAIR = 2
PIECES = 2
LANES = PAIR * DK


def tables(length):
    half = DK // 2
    frequency = (10000.0 ** (-np.arange(half) / half)).astype(np.float32)
    angles = (np.arange(length, dtype=np.float32)[:, None] * frequency[None, :]).astype(np.float64)
    cosine = np.tile(np.cos(angles), (1, 4)).astype(np.float32)
    sine = np.tile(np.sin(angles), (1, 4)).astype(np.float32)
    swap = np.zeros((LANES, LANES), np.float32)
    for lane in range(LANES):
        if lane % DK < half:
            swap[lane + half, lane] = -1.0
        else:
            swap[lane - half, lane] = 1.0
    return jnp.asarray(cosine), jnp.asarray(sine), jnp.asarray(swap, jnp.bfloat16)


def layer_kernel(
    S, Z, rate_hbm, cos_hbm, sin_hbm, swap_hbm, x_ref, wq_ref, wk_ref, wv_ref, wo_ref, out_ref,
    tok, ftok, wqkv, wo, acc, decay, qk, val, sc, nown, fown, nrm, oacc, cos_ref, sin_ref, swap_ref, rate_ref,
    lsem, send, tR, rR, zR, fR, gR, qR, qpR, oR, xR, iR, jR, dR, opR, nR, hR,
):
    s = lax.axis_index("sp")
    d = lax.axis_index("dp")
    z, c = d // CORES, d % CORES
    rows, model = x_ref.shape
    length = S * rows
    depth = wq_ref.shape[0]
    heads = rate_hbm.shape[1]
    qc, vc = heads * DK, heads * DV
    wide_v = PAIR * DV
    oc = wo.shape[3]
    step_rows = depth // PIECES
    half_model = model // 2
    sx = s + 1 - 2 * (s % 2)
    sy = (s + 2) % 4
    sd = (sx + 2) % 4
    end = (z == 0) | (z == Z - 1)
    mid = jnp.logical_not(end)

    near, across, mirror = z + 1 - 2 * (z % 2), (z + 2) % Z, Z - 1 - z
    partner = {"dp": z * CORES + 1 - c}
    to_near, to_mirror = {"dp": near * CORES + c}, {"dp": mirror * CORES + c}

    def remote(src, send_at, recv, device, dst=None):
        return pltpu.make_async_remote_copy(
            src_ref=src, dst_ref=src if dst is None else dst, send_sem=send.at[send_at], recv_sem=recv,
            device_id=device, device_id_type=MESH,
        )

    def local(src, dst, at):
        return pltpu.make_async_copy(src, dst, lsem.at[at])

    def weight_copies(group):
        def part(ref, at, size, to):
            cols = pl.ds(pl.multiple_of(at + group * size, size), size)
            return local(ref.at[:, cols], wqkv.at[d, group, :, pl.ds(to, size)], group)

        return [
            part(wq_ref, s * qc, LANES, 0), part(wk_ref, s * qc, LANES, LANES),
            part(wv_ref, s * vc, wide_v, 2 * LANES),
        ]

    def quarter_copy(at, sem):
        return local(wo_ref.at[:, pl.ds(pl.multiple_of(at * oc, oc), oc)], wo.at[d, at], sem)

    def local_wait(ref, at):
        local(ref, ref, at).wait()

    local_c = [
        local(rate_hbm, rate_ref, 5), local(cos_hbm, cos_ref, 6),
        local(sin_hbm, sin_ref, 7), local(swap_hbm, swap_ref, 8),
    ]
    for copy in (
        weight_copies(0) + [local(x_ref, tok.at[s], 2), quarter_copy(s, 3)] + weight_copies(1)
        + local_c[:1] + [quarter_copy(at, 4) for at in (sd, sx, sy)] + local_c[1:]
    ):
        copy.start()

    barrier = pltpu.get_barrier_semaphore()

    def greet(device):
        pl.semaphore_signal(barrier, inc=1, device_id=device, device_id_type=MESH)

    greet(to_near)
    pl.when(mid)(lambda: greet(to_mirror))
    for other in range(1, S):
        greet({"sp": (s + other) % S})
    greet(partner)
    pl.when(mid)(lambda: pl.semaphore_wait(barrier, S + 2))
    pl.when(end)(lambda: pl.semaphore_wait(barrier, S + 1))

    def q_copy(src, group, device):
        return remote(wqkv.at[src * CORES + c, group], 0, qR.at[src, group], device)

    def qp_copy(src, group):
        return remote(wqkv.at[src * CORES + c, group], 2, qpR.at[src, group], partner)

    def qp_wait(src, group):
        remote(wqkv.at[src * CORES + 1 - c, group], 2, qpR.at[src, group], partner).wait_recv()

    def o_piece(block, quarter, piece):
        return wo.at[block, quarter, pl.ds(piece * step_rows, step_rows)]

    def o_copy(src, piece, device):
        return remote(o_piece(src * CORES + c, s, piece), 1, oR.at[src, piece], device)

    def x_copy(src, extra, device):
        return remote(wo.at[src * CORES + c, (sd, sx, sy)[extra]], 1, xR.at[src, extra], device)

    def op_copy(src, quarter):
        return remote(wo.at[src * CORES + c, quarter], 3, opR.at[src], partner)

    def o_ready(src):
        remote(wo.at[src * CORES + 1 - c], 3, opR.at[src], partner).wait_recv()

    def i_copy(axis, src, piece, recv):
        return remote(o_piece(src * CORES + c, s, piece), 4, recv, {"sp": sx if axis == 0 else sy})

    def d_copy(src, piece):
        to, quarter = (sy, sx) if piece == 0 else (sx, sy)
        return remote(o_piece(src * CORES + c, quarter, piece), 5, dR.at[src], {"sp": to})

    def half_ref(buffer, block, half):
        return buffer.at[block, :, pl.ds(half * half_model, half_model)]

    def t_copy(buffer, axis, half, at, recv):
        return remote(half_ref(buffer, s, half), at, recv.at[axis, half], {"sp": sx if axis == 0 else sy})

    def t_wait(buffer, axis, half, recv):
        remote(half_ref(buffer, sx if axis == 0 else sy, half), 6, recv.at[axis, half], {"sp": sx}).wait_recv()

    def r_copy(buffer, half, at, recv):
        to, block = (sy, sx) if half == 0 else (sx, sy)
        return remote(half_ref(buffer, block, half), at, recv.at[half], {"sp": to})

    def r_wait(buffer, half, recv):
        remote(half_ref(buffer, sd, half), 6, recv.at[half], {"sp": sx}).wait_recv()

    def z_copy(half):
        return remote(half_ref(tok, s, half), 10, zR.at[half], to_near, dst=half_ref(ftok, s, half))

    def n_copy(head, to):
        return remote(
            nown.at[head, pl.ds(pl.multiple_of(to * rows, rows), rows)], 7, nR.at[head // PAIR, s], {"sp": to},
            dst=nrm.at[s, :, pl.ds(head * DV, DV)],
        )

    def n_wait(group, j):
        ref = nrm.at[j, :, pl.ds(group * wide_v, wide_v)]
        remote(ref, 7, nR.at[group, j], {"sp": j}).wait_recv()

    def h_copy(inner, to):
        return remote(
            fown.at[inner, pl.ds(pl.multiple_of(to * rows, rows), rows)], 8, nR.at[1, s],
            {"sp": to, "dp": near * CORES + c}, dst=nrm.at[s, :, pl.ds((PAIR + inner) * DV, DV)],
        )

    def decays(group):
        for head in range(group * PAIR, (group + 1) * PAIR):
            fast, slow = rate_ref[0, head], rate_ref[1, head]

            @pl.loop(0, S)
            def _(j):
                at = lax.broadcasted_iota(jnp.int32, (rows, length), 0) + j * rows
                gap = (at - lax.broadcasted_iota(jnp.int32, (rows, length), 1)).astype(jnp.float32)
                weight = jnp.exp(jnp.where(gap >= 0.0, gap * fast, gap * (-slow)))
                decay[head, pl.ds(pl.multiple_of(j * rows, rows), rows), :] = jnp.where(gap == 0.0, 2.0, weight)

    tile = 2 * LANES

    def project(src, slot, buffer=tok, first=False):
        group = min(slot, 1)
        wide = CORES * depth
        cols = pl.ds(pl.multiple_of(src * wide, wide), wide)
        for n in range(2):
            at = slice(n * tile, (n + 1) * tile)
            part = jnp.dot(
                buffer[:, :, cols].reshape(length, wide),
                wqkv[pl.ds(src * CORES, CORES), group, :, at].reshape(wide, tile),
                preferred_element_type=jnp.float32,
            )
            if first:
                acc[slot, :, at] = part
            else:
                acc[slot, :, at] += part

    def scores(slot):
        for part in range(2):
            at = slice(part * LANES, (part + 1) * LANES)
            flat = acc[slot, :, at].astype(jnp.bfloat16)
            turned = jnp.dot(flat, swap_ref[...], preferred_element_type=jnp.float32)
            qk[:, at] = (flat.astype(jnp.float32) * cos_ref[...] + turned * sin_ref[...]).astype(jnp.bfloat16)
        lane = lax.broadcasted_iota(jnp.int32, (length, LANES), 1)
        for inner in range(PAIR):
            query = qk[:, :LANES]
            query = jnp.where((lane // DK) == inner, query.astype(jnp.float32), 0.0).astype(jnp.bfloat16)
            for n in range(length // tile):
                at = slice(n * tile, (n + 1) * tile)
                part = lax.dot_general(
                    query, qk[at, LANES:], (((1,), (1,)), ((), ())), preferred_element_type=jnp.float32,
                )
                sc[inner, :, at] = (part * decay[min(slot, 1) * PAIR + inner, :, at]).astype(jnp.bfloat16)

    def spread(head):
        for to in (sd, sx, sy):
            n_copy(head, to).start()
        nrm[s, :, head * DV : (head + 1) * DV] = nown[head, pl.ds(pl.multiple_of(s * rows, rows), rows), :]

    def values(slot):
        val[...] = acc[slot, :, 2 * LANES :].astype(jnp.bfloat16)
        for inner in range(PAIR):
            ret = jnp.dot(sc[inner], val[:, inner * DV : (inner + 1) * DV], preferred_element_type=jnp.float32)
            centred = ret - jnp.mean(ret, axis=-1, keepdims=True)
            variance = jnp.mean(centred * centred, axis=-1, keepdims=True)
            normed = (centred * lax.rsqrt(variance + 1e-06)).astype(jnp.bfloat16)
            if slot < 2:
                nown[slot * PAIR + inner] = normed
                spread(slot * PAIR + inner)
            else:
                fown[inner] = normed
                for to in (sd, sx, sy, s):
                    h_copy(inner, to).start()

    def retain(slot):
        scores(slot)
        values(slot)

    def finish(units, first=False, last=False, foreign=False):
        for src, group in units:
            if foreign:
                n_wait(group, src)
            else:
                pl.when(src != s)(lambda: n_wait(group, src))
        for j in range(S):
            at = slice(j * oc, (j + 1) * oc)
            total = None if first else oacc[:, at]
            for src, group in units:
                part = jnp.dot(
                    nrm[src, :, group * wide_v : (group + 1) * wide_v], wo[src * CORES + group, j],
                    preferred_element_type=jnp.float32,
                )
                total = part if total is None else total + part
            if last:
                out_ref[:, at] = total.astype(out_ref.dtype)
            else:
                oacc[:, at] = total

    def sent(ref, at):
        remote(ref, at, hR.at[0], partner).wait_send()

    def q_step(src, group, device=None):
        q_copy(src, group, to_near).wait_recv()
        if device is not None:
            q_copy(src, group, device).start()
        qp_copy(src, group).start()

    def project_in(src, slot, first=False):
        qp_wait(src, slot)
        project(src, slot, first=first)

    def tokens_out():
        local_wait(tok.at[s], 2)
        for half in range(2):
            t_copy(tok, 0, half, 6, tR).start()
            t_copy(tok, 1, 1 - half, 6, tR).start()

    def tokens_relay(buffer, at, recv, onward, halves=(0, 1)):
        for half in halves:
            t_wait(buffer, half, half, recv)
            r_copy(buffer, half, at, onward).start()

    def tokens_in(buffer, recv, onward):
        t_wait(buffer, 0, 1, recv)
        t_wait(buffer, 1, 0, recv)
        for half in range(2):
            r_wait(buffer, half, onward)

    def run_end():
        def o_step(src):
            for piece in range(PIECES):
                o_copy(src, piece, to_near).wait_recv()
                i_copy(piece, src, piece, iR.at[piece, src]).start()
                i_copy(1 - piece, src, piece, jR.at[src]).start()
            op_copy(src, s).start()

        def o_relay(src):
            for piece in range(PIECES):
                block = o_piece(src * CORES + c, sx if piece == 0 else sy, piece)
                remote(block, 4, iR.at[piece, src], {"sp": sx}).wait_recv()
                d_copy(src, piece).start()

        def o_share(src):
            remote(wo.at[src * CORES + c, sx], 4, jR.at[src], {"sp": sx}).wait_recv()
            op_copy(src, sx).start()
            op_copy(src, sy).start()
            remote(wo.at[src * CORES + c, sd], 5, dR.at[src], {"sp": sx}).wait_recv()
            op_copy(src, sd).start()

        local_wait(wqkv.at[d, 0], 0)
        q_copy(z, 0, to_near).start()
        tokens_out()
        qp_copy(z, 0).start()
        local_wait(wo.at[d, s], 3)
        for piece in range(PIECES):
            o_copy(z, piece, to_near).start()
        for half in range(2):
            z_copy(half).start()
        local_wait(wqkv.at[d, 1], 1)
        q_copy(z, 1, to_near).start()
        local_wait(wo.at[pl.ds(0, S - 1), 0], 4)
        for extra in range(S - 1):
            x_copy(z, extra, to_near).start()
        for at in (s, sd, sx, sy):
            op_copy(z, at).start()
        local_c[0].wait()
        decays(0)
        tokens_relay(tok, 6, tR, rR)
        q_step(near, 0)
        o_step(near)
        for copy in local_c[1:]:
            copy.wait()
        tokens_in(tok, tR, rR)
        project_in(z, 0, True)
        project_in(near, 0)
        q_step(across, 0)
        o_relay(near)
        project_in(across, 0)
        q_step(mirror, 0)
        project_in(mirror, 0)
        retain(0)
        o_share(near)
        o_step(mirror)
        o_ready(z)
        o_ready(near)
        finish(((z, 0), (near, 0)), first=True)
        o_step(across)
        o_relay(mirror)
        o_share(mirror)
        o_relay(across)
        o_ready(mirror)
        finish(((mirror, 0),))
        o_share(across)
        o_ready(across)
        finish(((across, 0),))
        finish(((z, 1), (near, 1), (mirror, 1), (across, 1)), last=True, foreign=True)
        sent(wqkv.at[pl.ds(0, 2), 0], 0)
        sent(wo.at[pl.ds(0, S), 0], 1)
        sent(wqkv.at[pl.ds(0, Z), 0], 2)
        sent(wo.at[pl.ds(0, Z)], 3)
        sent(wo.at[pl.ds(0, Z - 1), pl.ds(0, 2)], 4)
        sent(wo.at[pl.ds(0, Z - 1), 0], 5)
        sent(tok.at[0], 10)
        sent(nown.at[pl.ds(0, PAIR), pl.ds(0, (S - 1) * rows)], 7)

    def run_mid():
        def o_step(src, device):
            for piece in range(PIECES):
                o_copy(src, piece, device).wait_recv()
                o_copy(src, piece, device).start()
            op_copy(src, s).start()

        def o_send(src):
            for piece in range(PIECES):
                i_copy(0, src, piece, jR.at[src]).start()
                i_copy(1, src, piece, jR.at[src]).start()

        def x_step(src, extra, device=None):
            x_copy(src, extra, to_near).wait_recv()
            if device is not None:
                x_copy(src, extra, device).start()
            op_copy(src, (sd, sx, sy)[extra]).start()

        def o_share(src):
            remote(wo.at[src * CORES + c, pl.ds(0, 2)], 4, jR.at[src], {"sp": sx}).wait_recv()
            op_copy(src, sx).start()
            op_copy(src, sy).start()

        def foreign(half):
            remote(half_ref(ftok, s, half), 10, zR.at[half], to_near).wait_recv()
            t_copy(ftok, 0, half, 9, fR).start()
            t_copy(ftok, 1, half, 9, fR).start()

        local_wait(wqkv.at[d, 0], 0)
        q_copy(z, 0, to_near).start()
        q_copy(z, 0, to_mirror).start()
        tokens_out()
        qp_copy(z, 0).start()
        local_wait(wo.at[d, s], 3)
        for piece in range(PIECES):
            o_copy(z, piece, to_near).start()
        local_wait(wqkv.at[d, 1], 1)
        qp_copy(z, 1).start()
        local_wait(wo.at[pl.ds(0, S - 1), 0], 4)
        for at in (s, sd, sx, sy):
            op_copy(z, at).start()
        local_c[0].wait()
        decays(0)
        tokens_relay(tok, 6, tR, rR)
        q_step(near, 0, to_mirror)
        q_step(mirror, 0, to_near)
        o_step(near, to_mirror)
        q_copy(z, 1, to_mirror).start()
        for piece in range(PIECES):
            o_copy(z, piece, to_mirror).start()
        q_step(across, 0, to_near)
        for copy in local_c[1:]:
            copy.wait()
        tokens_in(tok, tR, rR)
        foreign(0)
        project_in(z, 0, True)
        project_in(near, 0)
        project_in(mirror, 0)
        o_step(across, to_near)
        project_in(across, 0)
        foreign(1)
        retain(0)
        q_step(mirror, 1)
        tokens_relay(ftok, 9, fR, gR, (0,))
        o_step(mirror, to_near)
        decays(1)
        project_in(z, 1, True)
        project_in(mirror, 1)
        tokens_relay(ftok, 9, fR, gR, (1,))
        q_step(near, 1, to_mirror)
        x_copy(z, 0, to_mirror).start()
        project_in(near, 1)
        o_ready(z)
        finish(((z, 0),), first=True)
        x_step(near, 0, to_mirror)
        q_step(across, 1)
        tokens_in(ftok, fR, gR)
        o_send(across)
        o_send(mirror)
        project(z, 2, ftok, True)
        project(near, 2, ftok)
        project(mirror, 2, ftok)
        qp_wait(across, 1)
        project(across, 2, ftok)
        retain(2)
        project(across, 1)
        retain(1)
        x_step(near, 1)
        x_step(mirror, 0)
        o_share(across)
        o_share(mirror)
        x_step(near, 2)
        o_ready(mirror)
        finish(((mirror, 0), (mirror, 1), (z, 1)))
        x_step(across, 0)
        o_ready(near)
        o_ready(across)
        finish(((across, 0), (across, 1), (near, 0), (near, 1)), last=True)
        sent(wqkv.at[pl.ds(0, 7), 0], 0)
        sent(wo.at[pl.ds(0, 7), 0], 1)
        sent(wqkv.at[pl.ds(0, Z)], 2)
        sent(wo.at[pl.ds(0, Z)], 3)
        sent(wo.at[pl.ds(0, 2), pl.ds(0, 2)], 4)
        sent(fown, 8)
        sent(nown.at[:, pl.ds(0, (S - 1) * rows)], 7)
        sent(ftok.at[pl.ds(0, S - 1)], 9)

    pl.when(end)(run_end)
    pl.when(mid)(run_mid)
    sent(tok.at[pl.ds(0, S - 1)], 6)


def fused(S, Z, tokens, query_weight, key_weight, value_weight, output_weight, log_decay):
    rows, model = tokens.shape[1:]
    depth = query_weight.shape[0]
    heads = log_decay.shape[1]
    groups = heads // PAIR
    length = S * rows
    width = 2 * LANES + PAIR * DV
    oc = output_weight.shape[1] // S
    cosine, sine, swap = tables(length)
    anyplace = pl.BlockSpec(memory_space=pl.ANY)
    dma = pltpu.SemaphoreType.DMA
    bf, f32 = jnp.bfloat16, jnp.float32
    out = pl.pallas_call(
        functools.partial(layer_kernel, S, Z),
        out_shape=pltpu.VMEM((rows, output_weight.shape[1]), bf),
        in_specs=[anyplace] * 9,
        out_specs=pl.BlockSpec(memory_space=pltpu.VMEM),
        scratch_shapes=[
            pltpu.VMEM((S, rows, model), bf),
            pltpu.VMEM((S, rows, model), bf),
            pltpu.VMEM((Z * CORES, groups, depth, width), bf),
            pltpu.VMEM((Z * CORES, S, depth, oc), bf),
            pltpu.VMEM((groups + 1, length, width), f32),
            pltpu.VMEM((heads, length, length), f32),
            pltpu.VMEM((length, 2 * LANES), bf),
            pltpu.VMEM((length, PAIR * DV), bf),
            pltpu.VMEM((PAIR, length, length), bf),
            pltpu.VMEM((heads, length, DV), bf),
            pltpu.VMEM((PAIR, length, DV), bf),
            pltpu.VMEM((S, rows, heads * DV), bf),
            pltpu.VMEM((rows, S * oc), f32),
            pltpu.VMEM((length, LANES), f32), pltpu.VMEM((length, LANES), f32), pltpu.VMEM((LANES, LANES), bf),
            pltpu.SMEM((2, heads), f32),
            dma((9,)), dma((11,)), dma((2, 2)), dma((2,)), dma((2,)), dma((2, 2)), dma((2,)),
            dma((Z, groups)), dma((Z, groups)), dma((Z, PIECES)), dma((Z, 3)),
            dma((2, Z)), dma((Z,)), dma((Z,)), dma((Z,)), dma((groups, S)), dma((PAIR,)),
        ],
        compiler_params=pltpu.CompilerParams(
            collective_id=0, has_side_effects=True, vmem_limit_bytes=56 * 1024 * 1024
        ),
    )(log_decay, cosine, sine, swap, tokens[0], query_weight, key_weight, value_weight, output_weight)
    return out[None]


def solution(mesh):
    S, D = mesh.shape["sp"], mesh.shape["dp"]
    Z = D // CORES

    def layer(tokens, query_weight, key_weight, value_weight, output_weight, log_decay):
        rows = tokens.shape[1]
        depth = query_weight.shape[0]
        heads = log_decay.shape[1]
        fits = (
            S == 4 and Z == 4 and D == CORES * Z and S * rows == BLOCK and heads == CORES * PAIR
            and PAIR * DV == depth and rows % 128 == 0
        )
        args = (tokens, query_weight, key_weight, value_weight, output_weight, log_decay)
        return fused(S, Z, *args) if fits else shards(*args)

    placed = (
        P("dp", "sp", None),
        P("dp", None),
        P("dp", None),
        P("dp", None),
        P("dp", None),
        P(None, "sp"),
    )
    return jax.shard_map(
        layer, mesh=mesh, in_specs=placed, out_specs=P("dp", "sp", None), check_vma=False
    )
```

time: 69.3 us -> 61.4 us (0.89)
  Pallas kernels: 68.3 us -> 60 us
    pallas_call x1, Pallas kernels: 68.3 us -> 60 us  [fused(): pl.pallas_call(functools.partial(layer_kernel, S, Z), out_shape=pltpu.VME...]
where the time goes in v3:
time: 61.4 us; the launch traced here: 60.8 us
  Pallas kernels  60 us (98%)
  local copies, waits for them, and re-layouts  0.8 us (1%)
    pallas_call x1, Pallas kernels, fused(): pl.pallas_call(functools.partial(layer_kernel, S, Z), out_shape=pltpu.VME...  60 us

profile of v3, /device:TPU:0, one launch (start us, length us, event | category | flops | bytes accessed | tf_op | source)
XLA Modules:
  0.0 60.8 jit_solution(9146268079467220531)
XLA Ops:
  0.0 60.0 %shard_map.91 = bf16[128,2048]{1,0:T(8,128)(2,1)S(1)} custom-call(f32[2,4]{1,0:T(2,128)} %rate_hbm.1, f32[512,128]{1,0:T(8,128)} %constant.6.clone.cos_hbm, f32[512,128]{1,0:T(8,128)} %constant.7.clone.sin_hbm, bf16[128,128]{1,0:T(8,128)(2,1)} %constant.8.clone.swap_hbm, bf16[128,2048]{1,0:T(8,128)(2,1)} %bitcast.3, bf16[256,1024]{1,0:T(8,128)(2,1)} %wq_ref.1, ...), custom_call_target="tpu_custom_call" | custom-call | tf_op jit(solution)/shard_map/pallas_call | solution.py:613
  60.0 0.8 %copy.11 = bf16[1,128,2048]{2,1,0:T(8,128)(2,1)} copy(bf16[1,128,2048]{2,1,0:T(8,128)(2,1)S(1)} %bitcast.2) | data formatting | bytes 1048576

commit v4 on v3

--- a/solution.py
+++ b/solution.py
@@ -151,7 +151,7 @@
 def layer_kernel(
     S, Z, rate_hbm, cos_hbm, sin_hbm, swap_hbm, x_ref, wq_ref, wk_ref, wv_ref, wo_ref, out_ref,
     tok, ftok, wqkv, wo, acc, decay, qk, val, sc, nown, fown, nrm, oacc, cos_ref, sin_ref, swap_ref, rate_ref,
-    lsem, send, tR, rR, zR, fR, gR, qR, qpR, oR, xR, iR, jR, dR, opR, nR, hR,
+    lsem, send, tR, rR, qR, qpR, oR, xR, iR, jR, dR, opR, nR,
 ):
     s = lax.axis_index("sp")
     d = lax.axis_index("dp")
@@ -217,11 +217,11 @@
 
     greet(to_near)
     pl.when(mid)(lambda: greet(to_mirror))
-    for other in range(1, S):
-        greet({"sp": (s + other) % S})
+    greet({"sp": sx})
+    greet({"sp": sy})
     greet(partner)
-    pl.when(mid)(lambda: pl.semaphore_wait(barrier, S + 2))
-    pl.when(end)(lambda: pl.semaphore_wait(barrier, S + 1))
+    pl.when(mid)(lambda: pl.semaphore_wait(barrier, S + 1))
+    pl.when(end)(lambda: pl.semaphore_wait(barrier, S))
 
     def q_copy(src, group, device):
         return remote(wqkv.at[src * CORES + c, group], 0, qR.at[src, group], device)
@@ -239,7 +239,7 @@
         return remote(o_piece(src * CORES + c, s, piece), 1, oR.at[src, piece], device)
 
     def x_copy(src, extra, device):
-        return remote(wo.at[src * CORES + c, (sd, sx, sy)[extra]], 1, xR.at[src, extra], device)
+        return remote(wo.at[src * CORES + c, (sd, sx, sy)[extra]], 1, dR.at[extra] if extra else xR.at[src], device)
 
     def op_copy(src, quarter):
         return remote(wo.at[src * CORES + c, quarter], 3, opR.at[src], partner)
@@ -263,15 +263,15 @@
     def t_wait(buffer, axis, half, recv):
         remote(half_ref(buffer, sx if axis == 0 else sy, half), 6, recv.at[axis, half], {"sp": sx}).wait_recv()
 
-    def r_copy(buffer, half, at, recv):
+    def r_copy(buffer, half, at):
         to, block = (sy, sx) if half == 0 else (sx, sy)
-        return remote(half_ref(buffer, block, half), at, recv.at[half], {"sp": to})
-
-    def r_wait(buffer, half, recv):
-        remote(half_ref(buffer, sd, half), 6, recv.at[half], {"sp": sx}).wait_recv()
+        return remote(half_ref(buffer, block, half), at, rR.at[half] if buffer is tok else iR.at[half, 2], {"sp": to})
+
+    def r_wait(buffer, half):
+        remote(half_ref(buffer, sd, half), 6, rR.at[half] if buffer is tok else iR.at[half, 2], {"sp": sx}).wait_recv()
 
     def z_copy(half):
-        return remote(half_ref(tok, s, half), 10, zR.at[half], to_near, dst=half_ref(ftok, s, half))
+        return remote(half_ref(tok, s, half), 10, iR.at[half, 3], to_near, dst=half_ref(ftok, s, half))
 
     def n_copy(head, to):
         return remote(
@@ -359,8 +359,10 @@
         scores(slot)
         values(slot)
 
-    def finish(units, first=False, last=False, foreign=False):
+    def finish(units, first=False, last=False, foreign=False, waited=False):
         for src, group in units:
+            if waited:
+                continue
             if foreign:
                 n_wait(group, src)
             else:
@@ -380,7 +382,7 @@
                 oacc[:, at] = total
 
     def sent(ref, at):
-        remote(ref, at, hR.at[0], partner).wait_send()
+        remote(ref, at, rR.at[0], partner).wait_send()
 
     def q_step(src, group, device=None):
         q_copy(src, group, to_near).wait_recv()
@@ -398,16 +400,16 @@
             t_copy(tok, 0, half, 6, tR).start()
             t_copy(tok, 1, 1 - half, 6, tR).start()
 
-    def tokens_relay(buffer, at, recv, onward, halves=(0, 1)):
+    def tokens_relay(buffer, at, recv, halves=(0, 1)):
         for half in halves:
             t_wait(buffer, half, half, recv)
-            r_copy(buffer, half, at, onward).start()
-
-    def tokens_in(buffer, recv, onward):
+            r_copy(buffer, half, at).start()
+
+    def tokens_in(buffer, recv):
         t_wait(buffer, 0, 1, recv)
         t_wait(buffer, 1, 0, recv)
         for half in range(2):
-            r_wait(buffer, half, onward)
+            r_wait(buffer, half)
 
     def run_end():
         def o_step(src):
@@ -448,12 +450,12 @@
             op_copy(z, at).start()
         local_c[0].wait()
         decays(0)
-        tokens_relay(tok, 6, tR, rR)
+        tokens_relay(tok, 6, tR)
         q_step(near, 0)
         o_step(near)
         for copy in local_c[1:]:
             copy.wait()
-        tokens_in(tok, tR, rR)
+        tokens_in(tok, tR)
         project_in(z, 0, True)
         project_in(near, 0)
         q_step(across, 0)
@@ -469,14 +471,16 @@
         finish(((z, 0), (near, 0)), first=True)
         o_step(across)
         o_relay(mirror)
+        o_relay(across)
         o_share(mirror)
-        o_relay(across)
         o_ready(mirror)
         finish(((mirror, 0),))
         o_share(across)
+        finish(((z, 1), (near, 1), (mirror, 1)), foreign=True)
+        n_wait(1, across)
         o_ready(across)
-        finish(((across, 0),))
-        finish(((z, 1), (near, 1), (mirror, 1), (across, 1)), last=True, foreign=True)
+        pl.when(across != s)(lambda: n_wait(0, across))
+        finish(((across, 0), (across, 1)), last=True, waited=True)
         sent(wqkv.at[pl.ds(0, 2), 0], 0)
         sent(wo.at[pl.ds(0, S), 0], 1)
         sent(wqkv.at[pl.ds(0, Z), 0], 2)
@@ -510,9 +514,9 @@
             op_copy(src, sy).start()
 
         def foreign(half):
-            remote(half_ref(ftok, s, half), 10, zR.at[half], to_near).wait_recv()
-            t_copy(ftok, 0, half, 9, fR).start()
-            t_copy(ftok, 1, half, 9, fR).start()
+            remote(half_ref(ftok, s, half), 10, iR.at[half, 3], to_near).wait_recv()
+            t_copy(ftok, 0, half, 9, iR).start()
+            t_copy(ftok, 1, half, 9, iR).start()
 
         local_wait(wqkv.at[d, 0], 0)
         q_copy(z, 0, to_near).start()
@@ -529,7 +533,7 @@
             op_copy(z, at).start()
         local_c[0].wait()
         decays(0)
-        tokens_relay(tok, 6, tR, rR)
+        tokens_relay(tok, 6, tR)
         q_step(near, 0, to_mirror)
         q_step(mirror, 0, to_near)
         o_step(near, to_mirror)
@@ -539,7 +543,7 @@
         q_step(across, 0, to_near)
         for copy in local_c[1:]:
             copy.wait()
-        tokens_in(tok, tR, rR)
+        tokens_in(tok, tR)
         foreign(0)
         project_in(z, 0, True)
         project_in(near, 0)
@@ -549,20 +553,20 @@
         foreign(1)
         retain(0)
         q_step(mirror, 1)
-        tokens_relay(ftok, 9, fR, gR, (0,))
+        tokens_relay(ftok, 9, iR, (0,))
         o_step(mirror, to_near)
         decays(1)
         project_in(z, 1, True)
         project_in(mirror, 1)
-        tokens_relay(ftok, 9, fR, gR, (1,))
         q_step(near, 1, to_mirror)
         x_copy(z, 0, to_mirror).start()
+        tokens_relay(ftok, 9, iR, (1,))
         project_in(near, 1)
         o_ready(z)
         finish(((z, 0),), first=True)
         x_step(near, 0, to_mirror)
         q_step(across, 1)
-        tokens_in(ftok, fR, gR)
+        tokens_in(ftok, iR)
         o_send(across)
         o_send(mirror)
         project(z, 2, ftok, True)
@@ -576,14 +580,15 @@
         x_step(near, 1)
         x_step(mirror, 0)
         o_share(across)
+        x_step(near, 2)
+        x_step(across, 0)
         o_share(mirror)
-        x_step(near, 2)
-        o_ready(mirror)
-        finish(((mirror, 0), (mirror, 1), (z, 1)))
-        x_step(across, 0)
         o_ready(near)
         o_ready(across)
-        finish(((across, 0), (across, 1), (near, 0), (near, 1)), last=True)
+        finish(((near, 0), (across, 0)))
+        finish(((z, 1), (near, 1), (across, 1)))
+        o_ready(mirror)
+        finish(((mirror, 0), (mirror, 1)), last=True)
         sent(wqkv.at[pl.ds(0, 7), 0], 0)
         sent(wo.at[pl.ds(0, 7), 0], 1)
         sent(wqkv.at[pl.ds(0, Z)], 2)
@@ -631,9 +636,9 @@
             pltpu.VMEM((rows, S * oc), f32),
             pltpu.VMEM((length, LANES), f32), pltpu.VMEM((length, LANES), f32), pltpu.VMEM((LANES, LANES), bf),
             pltpu.SMEM((2, heads), f32),
-            dma((9,)), dma((11,)), dma((2, 2)), dma((2,)), dma((2,)), dma((2, 2)), dma((2,)),
-            dma((Z, groups)), dma((Z, groups)), dma((Z, PIECES)), dma((Z, 3)),
-            dma((2, Z)), dma((Z,)), dma((Z,)), dma((Z,)), dma((groups, S)), dma((PAIR,)),
+            dma((9,)), dma((11,)), dma((2, 2)), dma((2,)),
+            dma((Z, groups)), dma((Z, groups)), dma((Z, PIECES)), dma((Z,)),
+            dma((2, Z)), dma((Z,)), dma((Z,)), dma((Z,)), dma((groups, S)),
         ],
         compiler_params=pltpu.CompilerParams(
             collective_id=0, has_side_effects=True, vmem_limit_bytes=56 * 1024 * 1024

time: 61.4 us -> 59.1 us (0.963)
  Pallas kernels: 60 us -> 58.1 us
    pallas_call x1, Pallas kernels: 60 us -> 58.1 us  [fused(): pl.pallas_call(functools.partial(layer_kernel, S, Z), out_shape=pltpu.VME...]
where the time goes in v4:
time: 59.1 us; the launch traced here: 58.9 us
  Pallas kernels  58.1 us (98%)
  local copies, waits for them, and re-layouts  0.8 us (1%)
    pallas_call x1, Pallas kernels, fused(): pl.pallas_call(functools.partial(layer_kernel, S, Z), out_shape=pltpu.VME...  58.1 us

profile of v4, /device:TPU:0, one launch (start us, length us, event | category | flops | bytes accessed | tf_op | source)
XLA Modules:
  0.0 58.9 jit_solution(17263283019315163481)
XLA Ops:
  0.0 58.1 %shard_map.91 = bf16[128,2048]{1,0:T(8,128)(2,1)S(1)} custom-call(f32[2,4]{1,0:T(2,128)} %rate_hbm.1, f32[512,128]{1,0:T(8,128)} %constant.6.clone.cos_hbm, f32[512,128]{1,0:T(8,128)} %constant.7.clone.sin_hbm, bf16[128,128]{1,0:T(8,128)(2,1)} %constant.8.clone.swap_hbm, bf16[128,2048]{1,0:T(8,128)(2,1)} %bitcast.3, bf16[256,1024]{1,0:T(8,128)(2,1)} %wq_ref.1, ...), custom_call_target="tpu_custom_call" | custom-call | tf_op jit(solution)/shard_map/pallas_call | solution.py:618
  58.1 0.8 %copy.11 = bf16[1,128,2048]{2,1,0:T(8,128)(2,1)} copy(bf16[1,128,2048]{2,1,0:T(8,128)(2,1)S(1)} %bitcast.2) | data formatting | bytes 1048576
